TPU v7x, 32 devices: a whole 2x2x4 slice. The times are simulated.
32 devices in a mesh: fs: 8 (over z, x), tp: 4 (over y, core).
Axes of the slice: x: 2, y: 2, z: 4, core: 2. Of those that a mesh axis runs over, the one named last changes fastest.
Arguments:
- tokens: bfloat16 [1024, 2048], P('fs', 'tp'), may hold values from -6 to 6
- routes: int32 [1024, 2], P('fs'), may hold values from 0 to 3, all different within a row; in each aligned block of 128 rows (0 to 127, 128 to 255, ...) at most 96 rows name the same one
- route_weight: float32 [1024, 2], P('fs'), may hold values from 0.1 to 1
- norm_gain: float32 [2048], P('fs'), may hold values from 0.1 to 1.9
- expert_gate: float32 [4, 2048, 512], P(None, 'fs', 'tp'), may hold values from -0.125 to 0.125
- expert_up: float32 [4, 2048, 512], P(None, 'fs', 'tp'), may hold values from -0.125 to 0.125
- expert_down: float32 [4, 2048, 512], P(None, 'fs', 'tp'), may hold values from -0.25 to 0.25
- shared_gate: float32 [2048, 512], P('fs', 'tp'), may hold values from -0.125 to 0.125
- shared_up: float32 [2048, 512], P('fs', 'tp'), may hold values from -0.125 to 0.125
- shared_down: float32 [512, 2048], P('tp', 'fs'), may hold values from -0.25 to 0.25
Outputs:
- mixed: bfloat16 [1024, 2048], P('fs', 'tp')
- gate_sampler: bfloat16 [8, 2048, 256], P('fs', None, 'tp')
- up_sampler: bfloat16 [8, 2048, 256], P('fs', None, 'tp')
- down_sampler: bfloat16 [8, 2048, 256], P('fs', 'tp')
- shared_gate_out: bfloat16 [2048, 512], P(None, 'tp')
- shared_up_out: bfloat16 [2048, 512], P(None, 'tp')
- shared_down_out: bfloat16 [512, 2048], P('tp')
Inputs may be any that keep to these rules, and one draw needn't show every extreme that they name: `routes`: each row names 2 different experts. In each aligned block of 128 rows no expert is named by more than 96 rows, a bound that some block reaches.
All inputs are finite; a program needn't handle non-finite values.
Results may differ from a plain program's by a relative error of at most 0.009.
Values may be sent and summed in bfloat16 or wider, within the bound.
No kernel may reach another device: no remote copies, remote signals or barrier semaphores. Data moves between devices by JAX's collectives and lax.ppermute only.
A program may use at most 64 MiB of HBM per device.

v0:
```python
import jax
import jax.numpy as jnp
from jax import lax
from jax.sharding import PartitionSpec as P

EPS = 1e-06


def to_owners(matrix, expert_count, unit_count):
    row_share = matrix.shape[1]
    return (
        matrix.reshape(expert_count, row_share, 2, unit_count)
        .transpose(0, 2, 1, 3)
        .reshape(2 * expert_count, row_share, unit_count)
    )


def on_device(
    tokens,
    routes,
    route_weight,
    norm_gain,
    expert_gate,
    expert_up,
    expert_down,
    shared_gate,
    shared_up,
    shared_down,
):
    fs_count = lax.axis_size("fs")
    tp_count = lax.axis_size("tp")
    expert_count, row_share, col_share = expert_gate.shape
    unit_count = col_share // 2
    model_width = row_share * fs_count
    quarter = model_width // tp_count
    tok_count, pick_count = routes.shape
    capacity = 2 * ((3 * tok_count * pick_count + 4 * expert_count - 1) // (4 * expert_count))
    slot_count = fs_count * capacity
    row_gain = norm_gain[None, :, None]
    gate_owned = to_owners((expert_gate * row_gain).astype(jnp.bfloat16), expert_count, unit_count)
    up_owned = to_owners((expert_up * row_gain).astype(jnp.bfloat16), expert_count, unit_count)
    gate_new, up_new = (
        lax.all_to_all(gate_owned, "fs", split_axis=0, concat_axis=1, tiled=True),
        lax.all_to_all(up_owned, "fs", split_axis=0, concat_axis=1, tiled=True),
    )
    down_owned = to_owners(expert_down.astype(jnp.bfloat16), expert_count, unit_count)
    down_new = lax.all_to_all(
        lax.all_to_all(down_owned, "fs", split_axis=0, concat_axis=1, tiled=True),
        "tp",
        split_axis=1,
        concat_axis=2,
        tiled=True,
    )
    shared_gate_new, shared_up_new, shared_down_new = (
        lax.all_gather(
            (shared_gate * norm_gain[:, None]).astype(jnp.bfloat16), "fs", axis=0, tiled=True
        ),
        lax.all_gather(
            (shared_up * norm_gain[:, None]).astype(jnp.bfloat16), "fs", axis=0, tiled=True
        ),
        lax.all_gather(shared_down.astype(jnp.bfloat16), "fs", axis=1, tiled=True),
    )
    gathered = lax.all_gather(tokens, "tp", axis=1, tiled=True)
    tokens_wide = gathered.astype(jnp.float32)
    normed = (
        tokens_wide * lax.rsqrt(jnp.mean(tokens_wide * tokens_wide, axis=1, keepdims=True) + EPS)
    ).astype(jnp.bfloat16)
    shared_act = jnp.dot(normed, shared_gate_new, preferred_element_type=jnp.float32)
    shared_lin = jnp.dot(normed, shared_up_new, preferred_element_type=jnp.float32)
    shared_hidden = (jax.nn.silu(shared_act) * shared_lin).astype(jnp.bfloat16)
    shared_term = jnp.dot(shared_hidden, shared_down_new, preferred_element_type=jnp.float32)
    shared_sum = lax.psum_scatter(
        shared_term.astype(jnp.bfloat16), "tp", scatter_dimension=1, tiled=True
    ).astype(jnp.float32)
    assigned = routes.reshape(-1)
    onehot = (assigned[:, None] == jnp.arange(expert_count, dtype=jnp.int32)[None, :]).astype(
        jnp.int32
    )
    earlier = jnp.cumsum(onehot, axis=0) - onehot
    position = jnp.sum(earlier * onehot, axis=1)
    slot_index = assigned * capacity + position
    token_index = jnp.arange(tok_count * pick_count, dtype=jnp.int32) // pick_count
    slot_token = (
        jnp.full((expert_count * capacity,), tok_count, jnp.int32).at[slot_index].set(token_index)
    )
    padded = jnp.concatenate([normed, jnp.zeros((1, model_width), jnp.bfloat16)], axis=0)
    own_part = lax.dynamic_slice_in_dim(padded, lax.axis_index("tp") * quarter, quarter, 1)
    outgoing = jnp.repeat(
        own_part[slot_token].reshape(expert_count, capacity, quarter), 2, axis=0
    ).reshape(slot_count, quarter)
    arrived = lax.all_to_all(outgoing, "fs", split_axis=0, concat_axis=0, tiled=True)
    portion = lax.all_gather(arrived, "tp", axis=1, tiled=True)
    gate_rows = gate_new[0]
    up_rows = up_new[0]
    gate_act = jnp.dot(portion, gate_rows, preferred_element_type=jnp.float32)
    up_act = jnp.dot(portion, up_rows, preferred_element_type=jnp.float32)
    hidden = (jax.nn.silu(gate_act) * up_act).astype(jnp.bfloat16)
    down_cols = down_new[0]
    half_sum = lax.dot_general(
        lax.all_gather(hidden, "tp", axis=1, tiled=True),
        down_cols,
        (((1,), (1,)), ((), ())),
        preferred_element_type=jnp.float32,
    )
    returned = lax.all_to_all(
        half_sum.astype(jnp.bfloat16), "fs", split_axis=0, concat_axis=0, tiled=True
    )
    pair_sum = jnp.sum(
        returned.astype(jnp.float32).reshape(expert_count, 2, capacity, quarter), axis=1
    ).reshape(expert_count * capacity, quarter)
    gathered_slots = pair_sum[slot_index].reshape(tok_count, pick_count, quarter)
    routed = jnp.sum(gathered_slots * route_weight[:, :, None], axis=1)
    mixed = (shared_sum + routed).astype(jnp.bfloat16)
    return (mixed, gate_new, up_new, down_new, shared_gate_new, shared_up_new, shared_down_new)


def solution(mesh):
    in_specs = (
        P("fs", "tp"),
        P("fs", None),
        P("fs", None),
        P("fs"),
        P(None, "fs", "tp"),
        P(None, "fs", "tp"),
        P(None, "fs", "tp"),
        P("fs", "tp"),
        P("fs", "tp"),
        P("tp", "fs"),
    )
    out_specs = (
        P("fs", "tp"),
        P("fs", None, "tp"),
        P("fs", None, "tp"),
        P("fs", "tp", None),
        P(None, "tp"),
        P(None, "tp"),
        P("tp", None),
    )
    return jax.shard_map(
        on_device, mesh=mesh, in_specs=in_specs, out_specs=out_specs, check_vma=False
    )
```

profile of v0, /device:TPU:0, one launch (start us, length us, event | category | flops | bytes accessed | tf_op | source)
XLA Modules:
  0.0 257.9 jit_solution(7877371888522557811)
XLA Ops:
  7.2 0.8 copy.45
  8.0 0.1 eq.29
  8.1 0.1 eq.25
  8.3 0.7 broadcast_multiply_fusion
  9.0 8.9 %all_gather.18 = bf16[128,2048]{1,0:T(8,128)(2,1)S(1)} all-gather(bf16[128,512]{1,0:T(8,128)(2,1)} %param.10), channel_id=1, replica_groups=mesh['fs'=8,'tp'=4] {'tp'}, dimensions={1}, use_global_device_ids=true | all-gather | bytes 655360 | tf_op jit(solution)/shard_map/all_gather | solution.py:63
  17.8 0.2 fusion.2
  18.0 0.2 fusion.3
  18.2 1.2 reduce-window.6
  19.5 0.1 copy.47
  19.8 0.1 copy.44
  20.0 0.1 mul.94
  20.1 1.4 scatter_custom_fusion
  21.6 2.1 gather_fusion
  23.8 26.3 %all_to_all.75 = bf16[8,96,512]{2,1,0:T(8,128)(2,1)} all-to-all(bf16[8,96,512]{2,1,0:T(8,128)(2,1)S(1)} %bitcast.62), channel_id=1, replica_groups=mesh['fs'=8,'tp'=4] {'fs'}, dimensions={0} | all-to-all | bytes 1572864 | tf_op jit(solution)/shard_map/all_to_all | solution.py:91
  50.2 0.2 multiply_convert_fusion.1
  50.3 0.2 fusion.17
  50.6 0.1 pad_maximum_fusion
  50.7 0.9 copy.50
  51.6 3.6 %all-to-all-start.1 = ((bf16[8,256,64]{1,2,0:T(8,128)(2,1)}), bf16[8,256,64]{1,2,0:T(8,128)(2,1)S(1)}, u32[]{:S(2)}, u32[]{:S(2)}) async-start(bf16[8,256,64]{1,2,0:T(8,128)(2,1)} %copy.50), calls=%async_computation.2 | async-start | bytes 524288 | tf_op jit(solution)/shard_map/all_to_all | solution.py:43
  55.3 0.1 fusion.16
  55.4 0.1 pad_maximum_fusion.2
  55.5 0.9 copy.56
  56.4 7.8 %all-to-all-done.1 = bf16[8,256,64]{1,2,0:T(8,128)(2,1)S(1)} async-done(((bf16[8,256,64]{1,2,0:T(8,128)(2,1)}), bf16[8,256,64]{1,2,0:T(8,128)(2,1)S(1)}, u32[]{:S(2)}, u32[]{:S(2)}) %all-to-all-start.1) | async-done | bytes 262176 | tf_op jit(solution)/shard_map/all_to_all | solution.py:43
  64.2 3.6 %all-to-all-start.3 = ((bf16[8,256,64]{1,2,0:T(8,128)(2,1)}), bf16[8,256,64]{1,2,0:T(8,128)(2,1)S(1)}, u32[]{:S(2)}, u32[]{:S(2)}) async-start(bf16[8,256,64]{1,2,0:T(8,128)(2,1)} %copy.56), calls=%async_computation.4 | async-start | bytes 524288 | tf_op jit(solution)/shard_map/all_to_all | solution.py:48
  67.8 0.1 pad_maximum_fusion.1
  67.9 0.9 copy.53
  68.8 7.6 %all-to-all-done.3 = bf16[8,256,64]{1,2,0:T(8,128)(2,1)S(1)} async-done(((bf16[8,256,64]{1,2,0:T(8,128)(2,1)}), bf16[8,256,64]{1,2,0:T(8,128)(2,1)S(1)}, u32[]{:S(2)}, u32[]{:S(2)}) %all-to-all-start.3) | async-done | bytes 262176 | tf_op jit(solution)/shard_map/all_to_all | solution.py:48
  76.4 3.6 %all-to-all-start.2 = ((bf16[8,256,64]{1,2,0:T(8,128)(2,1)}), bf16[8,256,64]{1,2,0:T(8,128)(2,1)S(1)}, u32[]{:S(2)}, u32[]{:S(2)}) async-start(bf16[8,256,64]{1,2,0:T(8,128)(2,1)} %copy.53), calls=%async_computation.3 | async-start | bytes 524288 | tf_op jit(solution)/shard_map/all_to_all | solution.py:44
  80.1 33.5 %all_gather.19 = bf16[2048,128]{1,0:T(8,128)(2,1)S(1)} all-gather(bf16[256,128]{1,0:T(8,128)(2,1)S(1)} %get-tuple-element.34), channel_id=1, replica_groups=mesh['fs'=8,'tp'=4] {'fs'}, dimensions={0}, use_global_device_ids=true | all-gather | bytes 589824 | tf_op jit(solution)/shard_map/all_gather | solution.py:55
  113.6 0.3 copy.72
  113.9 0.3 reshape.148
  114.2 0.5 broadcast.90
  114.7 11.5 %reduce = bf16[2048,64]{1,0:T(8,128)(2,1)S(1)} reduce(bf16[2048,1,64]{2,1,0:T(2,128)(2,1)S(1)} %bitcast.60, bf16[]{:T(256)} %broadcast.90), dimensions={1}, to_apply=%bitcast.45.reduce_sub_computation | reduce | bytes 524290
  126.2 1.1 reshape.151
  127.3 3.4 %all-to-all-start.4 = ((bf16[4,2,16384]{2,1,0:T(2,128)(2,1)}), bf16[4,2,16384]{2,1,0:T(2,128)(2,1)S(1)}, u32[]{:S(2)}, u32[]{:S(2)}) async-start(bf16[4,2,16384]{2,1,0:T(2,128)(2,1)} %reshape.151), calls=%async_computation.5 | async-start | bytes 524288 | tf_op jit(solution)/shard_map/all_to_all | solution.py:47
  130.8 31.5 %all_gather.20 = bf16[2048,128]{1,0:T(8,128)(2,1)S(1)} all-gather(bf16[256,128]{1,0:T(8,128)(2,1)S(1)} %get-tuple-element.35), channel_id=1, replica_groups=mesh['fs'=8,'tp'=4] {'fs'}, dimensions={0}, use_global_device_ids=true | all-gather | bytes 589824 | tf_op jit(solution)/shard_map/all_gather | solution.py:58
  162.3 0.7 copy.74
  163.0 0.7 copy.75
  163.7 0.6 reshape.152
  164.4 0.6 copy.59
  165.0 0.2 all_to_all.62
  165.3 3.1 %fusion.20 = f32[768,64]{0,1:T(8,128)S(1)} fusion(bf16[768,2048]{1,0:T(8,128)(2,1)} %all-gather.2.cloned.1.call-done, bf16[2048,64]{0,1:T(8,128)(2,1)} %bitcast.71), kind=kOutput, calls=%fused_computation.54 | convolution fusion | flops 201326592 | bytes 3604480 | tf_op jit(solution)/shard_map/dot_general | solution.py:95
  168.4 1.1 fusion
  169.5 7.3 %all_gather.23 = bf16[768,256]{0,1:T(8,128)(2,1)S(1)} all-gather(bf16[768,64]{0,1:T(8,128)(2,1)S(1)} %fusion), channel_id=1, replica_groups=mesh['fs'=8,'tp'=4] {'tp'}, dimensions={1}, use_global_device_ids=true | all-gather | bytes 491520 | tf_op jit(solution)/shard_map/all_gather | solution.py:100
  176.7 1.3 convolution_convert_fusion.1
  178.0 4.3 %all-to-all-start.5 = ((bf16[8,96,512]{2,1,0:T(8,128)(2,1)}), bf16[8,96,512]{2,1,0:T(8,128)(2,1)}, u32[]{:S(2)}, u32[]{:S(2)}) async-start(bf16[8,96,512]{2,1,0:T(8,128)(2,1)} %bitcast.12), calls=%async_computation.6 | async-start | bytes 1572864 | tf_op jit(solution)/shard_map/all_to_all | solution.py:105
  182.4 43.3 %all_gather.21 = bf16[128,2048]{1,0:T(8,128)(2,1)S(1)} all-gather(bf16[128,256]{1,0:T(8,128)(2,1)S(1)} %convert_element_type.61), channel_id=1, replica_groups=mesh['fs'=8,'tp'=4] {'fs'}, dimensions={1}, use_global_device_ids=true | all-gather | bytes 589824 | tf_op jit(solution)/shard_map/all_gather | solution.py:61
  225.7 0.3 fusion.19
  226.0 1.3 convolution_convert_fusion
  227.4 0.1 copy.61
  227.5 0.2 copy.51
  227.7 0.8 all_to_all.66
  228.5 0.1 copy.54
  228.6 0.8 all_to_all.67
  229.5 0.8 copy.65
  230.3 1.4 convert_reduce_fusion
  231.7 1.0 gather_fusion.1
  232.6 0.3 reshape.121
  233.0 0.7 multiply_reduce_fusion
  233.7 13.4 %reduce-scatter.2.cloned.1.call-done = bf16[128,512]{1,0:T(8,128)(2,1)} async-done(((bf16[128,2048]{1,0:T(8,128)(2,1)}), bf16[128,512]{1,0:T(8,128)(2,1)}) %reduce-scatter.2.cloned.1.call-update) | async-done | bytes 131088 | tf_op jit(solution)/shard_map/reduce_scatter | solution.py:72
  247.1 1.6 add_convert_fusion
  248.7 0.8 copy.81
  249.5 0.8 copy.82
  250.3 0.8 copy.83
  (47 shorter events, 0.8 us)
Async XLA Ops:
  7.2 158.1 %all-gather.2.cloned.1.call-start = ((), (), s32[]{:S(2)}) async-start(), calls=%async_computation.8 | async-start | bytes 3932160 | tf_op jit(solution)/shard_map/all_gather | solution.py:92
  21.6 28.5 %copy-start.2 = (f32[4,256,128]{2,1,0:T(8,128)S(1)}, f32[4,256,128]{2,1,0:T(8,128)}, u32[]{:S(2)}) copy-start(f32[4,256,128]{2,1,0:T(8,128)} %param.14) | copy-start | bytes 1572868
  21.6 28.5 %copy-start.3 = (f32[4,256,128]{2,1,0:T(8,128)S(1)}, f32[4,256,128]{2,1,0:T(8,128)}, u32[]{:S(2)}) copy-start(f32[4,256,128]{2,1,0:T(8,128)} %param.15) | copy-start | bytes 1572868
  21.6 28.5 %copy-start.8 = (f32[256]{0:T(256)S(1)}, f32[256]{0:T(256)}, u32[]{:S(2)}) copy-start(f32[256]{0:T(256)} %param.13) | copy-start | bytes 3076
  50.1 5.1 %copy-start.1 = (f32[4,256,128]{2,1,0:T(8,128)S(1)}, f32[4,256,128]{2,1,0:T(8,128)}, u32[]{:S(2)}) copy-start(f32[4,256,128]{2,1,0:T(8,128)} %param.16) | copy-start | bytes 1572868
  51.6 12.6 %all-to-all-start.1 = ((bf16[8,256,64]{1,2,0:T(8,128)(2,1)}), bf16[8,256,64]{1,2,0:T(8,128)(2,1)S(1)}, u32[]{:S(2)}, u32[]{:S(2)}) async-start(bf16[8,256,64]{1,2,0:T(8,128)(2,1)} %copy.50), calls=%async_computation.2 | async-start | bytes 524288 | tf_op jit(solution)/shard_map/all_to_all | solution.py:43
  55.2 13.6 %copy-start.7 = (f32[128,256]{1,0:T(8,128)S(1)}, f32[128,256]{1,0:T(8,128)}, u32[]{:S(2)}) copy-start(f32[128,256]{1,0:T(8,128)} %param.19) | copy-start | bytes 393220
  55.3 24.8 %copy-start.5 = (f32[256,128]{1,0:T(8,128)S(1)}, f32[256,128]{1,0:T(8,128)}, u32[]{:S(2)}) copy-start(f32[256,128]{1,0:T(8,128)} %param.17) | copy-start | bytes 393220
  55.3 24.7 %copy-start.6 = (f32[256,128]{1,0:T(8,128)S(1)}, f32[256,128]{1,0:T(8,128)}, u32[]{:S(2)}) copy-start(f32[256,128]{1,0:T(8,128)} %param.18) | copy-start | bytes 393220
  64.2 12.2 %all-to-all-start.3 = ((bf16[8,256,64]{1,2,0:T(8,128)(2,1)}), bf16[8,256,64]{1,2,0:T(8,128)(2,1)S(1)}, u32[]{:S(2)}, u32[]{:S(2)}) async-start(bf16[8,256,64]{1,2,0:T(8,128)(2,1)} %copy.56), calls=%async_computation.4 | async-start | bytes 524288 | tf_op jit(solution)/shard_map/all_to_all | solution.py:48
  76.4 50.9 %all-to-all-start.2 = ((bf16[8,256,64]{1,2,0:T(8,128)(2,1)}), bf16[8,256,64]{1,2,0:T(8,128)(2,1)S(1)}, u32[]{:S(2)}, u32[]{:S(2)}) async-start(bf16[8,256,64]{1,2,0:T(8,128)(2,1)} %copy.53), calls=%async_computation.3 | async-start | bytes 524288 | tf_op jit(solution)/shard_map/all_to_all | solution.py:44
  127.3 36.4 %all-to-all-start.4 = ((bf16[4,2,16384]{2,1,0:T(2,128)(2,1)}), bf16[4,2,16384]{2,1,0:T(2,128)(2,1)S(1)}, u32[]{:S(2)}, u32[]{:S(2)}) async-start(bf16[4,2,16384]{2,1,0:T(2,128)(2,1)} %reshape.151), calls=%async_computation.5 | async-start | bytes 524288 | tf_op jit(solution)/shard_map/all_to_all | solution.py:47
  165.0 3.4 %copy-start.4 = (bf16[8,8,8,256]{3,2,0,1:T(8,128)(2,1)S(1)}, bf16[8,8,8,256]{3,2,0,1:T(8,128)(2,1)}, u32[]{:S(2)}) copy-start(bf16[8,8,8,256]{3,2,0,1:T(8,128)(2,1)} %copy.75) | copy-start | bytes 786436
  165.2 3.1 %copy-start = (bf16[768,2048]{1,0:T(8,128)(2,1)S(1)}, bf16[768,2048]{1,0:T(8,128)(2,1)}, u32[]{:S(2)}) copy-start(bf16[768,2048]{1,0:T(8,128)(2,1)} %all-gather.2.cloned.1.call-done) | copy-start | bytes 9437188
  178.0 49.4 %copy-start.9 = (f32[128,2]{0,1:T(2,128)S(1)}, f32[128,2]{0,1:T(2,128)}, u32[]{:S(2)}) copy-start(f32[128,2]{0,1:T(2,128)} %param.12) | copy-start | bytes 3076
  178.0 52.3 %all-to-all-start.5 = ((bf16[8,96,512]{2,1,0:T(8,128)(2,1)}), bf16[8,96,512]{2,1,0:T(8,128)(2,1)}, u32[]{:S(2)}, u32[]{:S(2)}) async-start(bf16[8,96,512]{2,1,0:T(8,128)(2,1)} %bitcast.12), calls=%async_computation.6 | async-start | bytes 1572864 | tf_op jit(solution)/shard_map/all_to_all | solution.py:105
  182.4 64.7 %reduce-scatter.2.cloned.1.call-start = ((), (), s32[]{:S(2)}) async-start(), calls=%async_computation.7 | async-start | bytes 655360 | tf_op jit(solution)/shard_map/reduce_scatter | solution.py:72
Sparse Core Ops, SparseCore 0:
  50.2 27.1 all-gather.1
  227.5 19.5 reduce-scatter.1
where the time goes:
time: 259 us; the launch traced here: 258 us
  blocking collectives  151 us (58%)
  waiting for transfers between devices  28.8 us (11%)
  local copies, waits for them, and re-layouts  19.9 us (8%)
  starting transfers between devices  18.7 us (7%)
  other arithmetic  18.2 us (7%)
  between operations  14.4 us (6%)
  matrix products  7.12 us (3%)
    all_gather x1, blocking collectives, on_device(): lax.all_gather(shared_down.astype(jnp.bfloat16), 'fs', axis=1, tiled=True)  43.3 us
    all_gather x1, blocking collectives, on_device(): lax.all_gather((shared_gate * norm_gain[:, None]).astype(jnp.bfloat16), '...  33.5 us
    all_gather x1, blocking collectives, on_device(): lax.all_gather((shared_up * norm_gain[:, None]).astype(jnp.bfloat16), 'fs...  31.5 us
    all_to_all x1, blocking collectives, on_device(): lax.all_to_all(outgoing, 'fs', split_axis=0, concat_axis=0, tiled=True)  26.3 us
    reduce_scatter x1, waiting for transfers between devices, on_device(): lax.psum_scatter(shared_term.astype(jnp.bfloat16), 'tp', scatter_dimensio...  13.4 us
    unnamed x2, other arithmetic  11.6 us
    all_gather x1, blocking collectives, on_device(): gathered = lax.all_gather(tokens, 'tp', axis=1, tiled=True)  8.87 us
    all_to_all x1, waiting for transfers between devices, on_device(): lax.all_to_all(gate_owned, 'fs', split_axis=0, concat_axis=1, tiled=True)  7.75 us
  transfers between devices with their start and end apart: 7, of which 3 were waited for; matrix products, arithmetic and copies ran while one was open for 10% of the time, Pallas kernels for 0%

commit v1 on v0

--- a/solution.py
+++ b/solution.py
@@ -44,13 +44,19 @@
         lax.all_to_all(up_owned, "fs", split_axis=0, concat_axis=1, tiled=True),
     )
     down_owned = to_owners(expert_down.astype(jnp.bfloat16), expert_count, unit_count)
-    down_new = lax.all_to_all(
-        lax.all_to_all(down_owned, "fs", split_axis=0, concat_axis=1, tiled=True),
-        "tp",
-        split_axis=1,
-        concat_axis=2,
-        tiled=True,
-    )
+    value = lax.all_to_all(down_owned, "fs", split_axis=0, concat_axis=1, tiled=True)
+    ways, here = (lax.axis_size("tp"), lax.axis_index("tp"))
+    width = value.shape[1] // ways
+    shape = list(value.shape)
+    shape[1] = width
+    height = shape[2]
+    shape[2] = height * ways
+    down_new = jnp.zeros(shape, value.dtype)
+    for mask in range(ways):
+        part = lax.dynamic_slice_in_dim(value, (here ^ mask) * width, width, axis=1)
+        if mask:
+            part = lax.ppermute(part, "tp", [(d, d ^ mask) for d in range(ways)])
+        down_new = lax.dynamic_update_slice_in_dim(down_new, part, (here ^ mask) * height, axis=2)
     shared_gate_new, shared_up_new, shared_down_new = (
         lax.all_gather(
             (shared_gate * norm_gain[:, None]).astype(jnp.bfloat16), "fs", axis=0, tiled=True

time: 259 us -> 243 us (0.938)
  other arithmetic: 18.2 us -> 6.68 us
    unnamed x2 -> x1, other arithmetic: 11.6 us -> 0.07 us
    all_gather x1, blocking collectives: 33.5 us -> 43.3 us  [on_device(): lax.all_gather((shared_gate * norm_gain[:, None]).astype(jnp.bfloat16), '...]
    all_gather x1, blocking collectives: 43.3 us -> 33.7 us  [on_device(): lax.all_gather(shared_down.astype(jnp.bfloat16), 'fs', axis=1, tiled=True)]
    all_to_all x1, waiting for transfers between devices: 0.01 us -> 7.75 us  [on_device(): lax.all_to_all(up_owned, 'fs', split_axis=0, concat_axis=1, tiled=True)]
    all_to_all x1, waiting for transfers between devices: 7.75 us -> 0.01 us  [on_device(): lax.all_to_all(gate_owned, 'fs', split_axis=0, concat_axis=1, tiled=True)]
    all_to_all x1 -> x0, starting transfers between devices: 3.41 us -> none  [on_device(): lax.all_to_all(lax.all_to_all(down_owned, 'fs', split_axis=0, concat_axis...]
    unnamed x29 -> x25, local copies, waits for them, and re-layouts: 6.41 us -> 3.33 us
    dynamic_update_slice x0 -> x4, local copies, waits for them, and re-layouts: none -> 2.64 us  [on_device(): lax.dynamic_update_slice_in_dim(down_new, part, (here ^ mask) * height, a...]
  transfers between devices with their start and end apart: 7 -> 9, of which waited for: 3 -> 3; matrix products, arithmetic and copies ran while one was open for 10% -> 5% of each run, Pallas kernels for 0% -> 0%
where the time goes in v1:
time: 243 us
  blocking collectives  150 us (62%)
  waiting for transfers between devices  29.5 us (12%)
  local copies, waits for them, and re-layouts  18.1 us (7%)
  starting transfers between devices  17.1 us (7%)
  between operations  14.5 us (6%)
  matrix products  7.13 us (3%)
  other arithmetic  6.68 us (3%)
    all_gather x1, blocking collectives, on_device(): lax.all_gather((shared_gate * norm_gain[:, None]).astype(jnp.bfloat16), '...  43.3 us
    all_gather x1, blocking collectives, on_device(): lax.all_gather(shared_down.astype(jnp.bfloat16), 'fs', axis=1, tiled=True)  33.7 us
    all_gather x1, blocking collectives, on_device(): lax.all_gather((shared_up * norm_gain[:, None]).astype(jnp.bfloat16), 'fs...  31.5 us
    all_to_all x1, blocking collectives, on_device(): lax.all_to_all(outgoing, 'fs', split_axis=0, concat_axis=0, tiled=True)  26.3 us
    reduce_scatter x1, waiting for transfers between devices, on_device(): lax.psum_scatter(shared_term.astype(jnp.bfloat16), 'tp', scatter_dimensio...  14.2 us
    all_gather x1, blocking collectives, on_device(): gathered = lax.all_gather(tokens, 'tp', axis=1, tiled=True)  8.89 us
    all_to_all x1, waiting for transfers between devices, on_device(): lax.all_to_all(up_owned, 'fs', split_axis=0, concat_axis=1, tiled=True)  7.75 us
    all_to_all x1, waiting for transfers between devices, on_device(): lax.all_to_all(down_owned, 'fs', split_axis=0, concat_axis=1, tiled=True)  7.45 us
  transfers between devices with their start and end apart: 9, of which 3 were waited for; matrix products, arithmetic and copies ran while one was open for 5% of the time, Pallas kernels for 0%

profile of v1, /device:TPU:0, one launch (start us, length us, event | category | flops | bytes accessed | tf_op | source)
XLA Modules:
  0.0 242.7 jit_solution(5952156706258513152)
XLA Ops:
  7.2 0.7 broadcast_multiply_fusion
  7.9 0.8 copy.37
  8.7 0.1 eq.29
  8.8 0.1 eq.25
  9.0 8.9 %all_gather.18 = bf16[128,2048]{1,0:T(8,128)(2,1)S(1)} all-gather(bf16[128,512]{1,0:T(8,128)(2,1)} %param.10), channel_id=1, replica_groups=mesh['fs'=8,'tp'=4] {'tp'}, dimensions={1}, use_global_device_ids=true | all-gather | bytes 655360 | tf_op jit(solution)/shard_map/all_gather | solution.py:69
  17.9 0.2 fusion.2
  18.1 0.2 fusion.3
  18.2 0.1 copy.36
  18.3 0.1 mul.116
  18.5 1.2 reduce-window.6
  20.1 1.4 scatter_custom_fusion
  21.6 2.1 gather_fusion
  23.8 26.3 %all_to_all.57 = bf16[8,96,512]{2,1,0:T(8,128)(2,1)} all-to-all(bf16[8,96,512]{2,1,0:T(8,128)(2,1)S(1)} %bitcast.57), channel_id=1, replica_groups=mesh['fs'=8,'tp'=4] {'fs'}, dimensions={0} | all-to-all | bytes 1572864 | tf_op jit(solution)/shard_map/all_to_all | solution.py:97
  50.2 0.2 multiply_convert_fusion.1
  50.3 0.2 fusion.18
  50.6 0.1 pad_maximum_fusion.1
  50.7 0.9 copy.45
  51.6 3.6 %all-to-all-start.2 = ((bf16[8,256,64]{1,2,0:T(8,128)(2,1)}), bf16[8,256,64]{1,2,0:T(8,128)(2,1)S(1)}, u32[]{:S(2)}, u32[]{:S(2)}) async-start(bf16[8,256,64]{1,2,0:T(8,128)(2,1)} %copy.45), calls=%async_computation.3 | async-start | bytes 524288 | tf_op jit(solution)/shard_map/all_to_all | solution.py:44
  55.3 0.1 fusion.17
  55.5 0.1 pad_maximum_fusion.2
  55.6 0.9 copy.48
  56.5 7.8 %all-to-all-done.2 = bf16[8,256,64]{1,2,0:T(8,128)(2,1)S(1)} async-done(((bf16[8,256,64]{1,2,0:T(8,128)(2,1)}), bf16[8,256,64]{1,2,0:T(8,128)(2,1)S(1)}, u32[]{:S(2)}, u32[]{:S(2)}) %all-to-all-start.2) | async-done | bytes 262176 | tf_op jit(solution)/shard_map/all_to_all | solution.py:44
  64.2 3.6 %all-to-all-start.3 = ((bf16[8,256,64]{1,2,0:T(8,128)(2,1)}), bf16[8,256,64]{1,2,0:T(8,128)(2,1)S(1)}, u32[]{:S(2)}, u32[]{:S(2)}) async-start(bf16[8,256,64]{1,2,0:T(8,128)(2,1)} %copy.48), calls=%async_computation.4 | async-start | bytes 524288 | tf_op jit(solution)/shard_map/all_to_all | solution.py:47
  67.8 0.1 pad_maximum_fusion
  67.9 0.9 copy.42
  69.0 7.5 %all-to-all-done.3 = bf16[8,256,64]{1,2,0:T(8,128)(2,1)S(1)} async-done(((bf16[8,256,64]{1,2,0:T(8,128)(2,1)}), bf16[8,256,64]{1,2,0:T(8,128)(2,1)S(1)}, u32[]{:S(2)}, u32[]{:S(2)}) %all-to-all-start.3) | async-done | bytes 262176 | tf_op jit(solution)/shard_map/all_to_all | solution.py:47
  76.4 3.6 %all-to-all-start.1 = ((bf16[8,256,64]{1,2,0:T(8,128)(2,1)}), bf16[8,256,64]{1,2,0:T(8,128)(2,1)S(1)}, u32[]{:S(2)}, u32[]{:S(2)}) async-start(bf16[8,256,64]{1,2,0:T(8,128)(2,1)} %copy.42), calls=%async_computation.2 | async-start | bytes 524288 | tf_op jit(solution)/shard_map/all_to_all | solution.py:43
  80.0 33.7 %all_gather.21 = bf16[128,2048]{1,0:T(8,128)(2,1)S(1)} all-gather(bf16[128,256]{1,0:T(8,128)(2,1)S(1)} %convert_element_type.61), channel_id=1, replica_groups=mesh['fs'=8,'tp'=4] {'fs'}, dimensions={1}, use_global_device_ids=true | all-gather | bytes 589824 | tf_op jit(solution)/shard_map/all_gather | solution.py:67
  113.7 0.1 copy.49
  113.9 0.1 all_to_all.47
  114.0 0.7 constant_dynamic-slice_fusion
  114.6 1.1 collective-permute-start.1
  115.7 0.8 collective-permute-start.2
  116.5 31.5 %all_gather.20 = bf16[2048,128]{1,0:T(8,128)(2,1)S(1)} all-gather(bf16[256,128]{1,0:T(8,128)(2,1)S(1)} %get-tuple-element.18), channel_id=1, replica_groups=mesh['fs'=8,'tp'=4] {'fs'}, dimensions={0}, use_global_device_ids=true | all-gather | bytes 589824 | tf_op jit(solution)/shard_map/all_gather | solution.py:64
  148.0 0.1 copy.50
  148.2 0.5 dynamic_update_slice.12
  148.7 0.1 copy.51
  148.8 0.9 dynamic_update_slice.13
  149.7 0.1 copy.52
  149.9 0.4 dynamic_update_slice.14
  150.3 0.1 copy.53
  150.4 0.8 dynamic_update_slice.15
  151.3 3.1 %fusion.21 = f32[768,64]{0,1:T(8,128)S(1)} fusion(bf16[768,2048]{1,0:T(8,128)(2,1)} %all-gather.2.cloned.1.call-done, bf16[2048,64]{0,1:T(8,128)(2,1)S(1)} %bitcast.64), kind=kOutput, calls=%fused_computation.59 | convolution fusion | flops 201326592 | bytes 3604480 | tf_op jit(solution)/shard_map/dot_general | solution.py:101
  154.4 1.1 fusion
  155.5 6.1 %all_gather.23 = bf16[768,256]{0,1:T(8,128)(2,1)S(1)} all-gather(bf16[768,64]{0,1:T(8,128)(2,1)S(1)} %fusion), channel_id=1, replica_groups=mesh['fs'=8,'tp'=4] {'tp'}, dimensions={1}, use_global_device_ids=true | all-gather | bytes 491520 | tf_op jit(solution)/shard_map/all_gather | solution.py:106
  161.6 1.3 convolution_convert_fusion.1
  163.0 4.3 %all-to-all-start.4 = ((bf16[8,96,512]{2,1,0:T(8,128)(2,1)}), bf16[8,96,512]{2,1,0:T(8,128)(2,1)}, u32[]{:S(2)}, u32[]{:S(2)}) async-start(bf16[8,96,512]{2,1,0:T(8,128)(2,1)} %bitcast.11), calls=%async_computation.5 | async-start | bytes 1572864 | tf_op jit(solution)/shard_map/all_to_all | solution.py:111
  167.4 43.3 %all_gather.19 = bf16[2048,128]{1,0:T(8,128)(2,1)S(1)} all-gather(bf16[256,128]{1,0:T(8,128)(2,1)S(1)} %get-tuple-element.17), channel_id=1, replica_groups=mesh['fs'=8,'tp'=4] {'fs'}, dimensions={0}, use_global_device_ids=true | all-gather | bytes 589824 | tf_op jit(solution)/shard_map/all_gather | solution.py:61
  210.7 0.3 fusion.20
  211.0 1.3 convolution_convert_fusion
  212.3 0.1 copy.54
  212.5 0.2 copy.43
  212.6 0.8 all_to_all.50
  213.4 0.1 copy.46
  213.6 0.8 all_to_all.51
  214.4 1.4 convert_reduce_fusion
  215.8 1.0 gather_fusion.1
  216.7 0.3 reshape.120
  217.1 0.7 multiply_reduce_fusion
  217.8 14.2 %reduce-scatter.2.cloned.1.call-done = bf16[128,512]{1,0:T(8,128)(2,1)} async-done(((bf16[128,2048]{1,0:T(8,128)(2,1)}), bf16[128,512]{1,0:T(8,128)(2,1)}) %reduce-scatter.2.cloned.1.call-update) | async-done | bytes 131088 | tf_op jit(solution)/shard_map/reduce_scatter | solution.py:78
  231.9 1.6 add_convert_fusion
  233.5 0.8 copy.74
  234.3 0.8 copy.75
  235.1 0.8 copy.76
  (53 shorter events, 0.9 us)
Async XLA Ops:
  7.2 144.1 %all-gather.2.cloned.1.call-start = ((), (), s32[]{:S(2)}) async-start(), calls=%async_computation.7 | async-start | bytes 3932160 | tf_op jit(solution)/shard_map/all_gather | solution.py:98
  21.6 28.5 %copy-start.3 = (f32[4,256,128]{2,1,0:T(8,128)S(1)}, f32[4,256,128]{2,1,0:T(8,128)}, u32[]{:S(2)}) copy-start(f32[4,256,128]{2,1,0:T(8,128)} %param.14) | copy-start | bytes 1572868
  21.6 28.5 %copy-start.4 = (f32[4,256,128]{2,1,0:T(8,128)S(1)}, f32[4,256,128]{2,1,0:T(8,128)}, u32[]{:S(2)}) copy-start(f32[4,256,128]{2,1,0:T(8,128)} %param.15) | copy-start | bytes 1572868
  21.6 28.5 %copy-start.8 = (f32[256]{0:T(256)S(1)}, f32[256]{0:T(256)}, u32[]{:S(2)}) copy-start(f32[256]{0:T(256)} %param.13) | copy-start | bytes 3076
  50.2 5.1 %copy-start.2 = (f32[4,256,128]{2,1,0:T(8,128)S(1)}, f32[4,256,128]{2,1,0:T(8,128)}, u32[]{:S(2)}) copy-start(f32[4,256,128]{2,1,0:T(8,128)} %param.16) | copy-start | bytes 1572868
  51.6 12.6 %all-to-all-start.2 = ((bf16[8,256,64]{1,2,0:T(8,128)(2,1)}), bf16[8,256,64]{1,2,0:T(8,128)(2,1)S(1)}, u32[]{:S(2)}, u32[]{:S(2)}) async-start(bf16[8,256,64]{1,2,0:T(8,128)(2,1)} %copy.45), calls=%async_computation.3 | async-start | bytes 524288 | tf_op jit(solution)/shard_map/all_to_all | solution.py:44
  55.2 13.6 %copy-start.7 = (f32[128,256]{1,0:T(8,128)S(1)}, f32[128,256]{1,0:T(8,128)}, u32[]{:S(2)}) copy-start(f32[128,256]{1,0:T(8,128)} %param.19) | copy-start | bytes 393220
  55.2 13.6 %copy-start.5 = (f32[256,128]{1,0:T(8,128)S(1)}, f32[256,128]{1,0:T(8,128)}, u32[]{:S(2)}) copy-start(f32[256,128]{1,0:T(8,128)} %param.17) | copy-start | bytes 393220
  55.3 13.6 %copy-start.6 = (f32[256,128]{1,0:T(8,128)S(1)}, f32[256,128]{1,0:T(8,128)}, u32[]{:S(2)}) copy-start(f32[256,128]{1,0:T(8,128)} %param.18) | copy-start | bytes 393220
  64.2 12.2 %all-to-all-start.3 = ((bf16[8,256,64]{1,2,0:T(8,128)(2,1)}), bf16[8,256,64]{1,2,0:T(8,128)(2,1)S(1)}, u32[]{:S(2)}, u32[]{:S(2)}) async-start(bf16[8,256,64]{1,2,0:T(8,128)(2,1)} %copy.48), calls=%async_computation.4 | async-start | bytes 524288 | tf_op jit(solution)/shard_map/all_to_all | solution.py:47
  76.4 71.6 %all-to-all-start.1 = ((bf16[8,256,64]{1,2,0:T(8,128)(2,1)}), bf16[8,256,64]{1,2,0:T(8,128)(2,1)S(1)}, u32[]{:S(2)}, u32[]{:S(2)}) async-start(bf16[8,256,64]{1,2,0:T(8,128)(2,1)} %copy.42), calls=%async_computation.2 | async-start | bytes 524288 | tf_op jit(solution)/shard_map/all_to_all | solution.py:43
  114.6 34.0 %collective-permute-start = (bf16[1,512,64]{1,2,0:T(8,128)(2,1)}, bf16[1,512,64]{1,2,0:T(8,128)(2,1)S(1)}, u32[]{:S(2)}, u32[]{:S(2)}) collective-permute-start(bf16[1,512,64]{1,2,0:T(8,128)(2,1)} %get-tuple-element.9), channel_id=1, source_target_pairs={{0,1},{1,0},{2,3},{3,2},{4,5},{5,4},{6,7},{7,6},{8,9},{9,8},{10,11... | collective-permute-start | bytes 196616 | tf_op jit(solution)/shard_map/ppermute | solution.py:58
  114.6 35.1 %collective-permute-start.1 = (bf16[1,512,64]{1,2,0:T(8,128)(2,1)S(1)}, bf16[1,512,64]{1,2,0:T(8,128)(2,1)S(1)}, u32[]{:S(2)}, u32[]{:S(2)}) collective-permute-start(bf16[1,512,64]{1,2,0:T(8,128)(2,1)S(1)} %get-tuple-element.8), channel_id=1, source_target_pairs={{0,2},{1,3},{2,0},{3,1},{4,6},{5,7},{6,4},{7,5},{8,10},{9,11},{10,... | collective-permute-start | bytes 196616 | tf_op jit(solution)/shard_map/ppermute | solution.py:58
  115.7 34.6 %collective-permute-start.2 = (bf16[1,512,64]{1,2,0:T(8,128)(2,1)S(1)}, bf16[1,512,64]{1,2,0:T(8,128)(2,1)S(1)}, u32[]{:S(2)}, u32[]{:S(2)}) collective-permute-start(bf16[1,512,64]{1,2,0:T(8,128)(2,1)S(1)} %get-tuple-element.7), channel_id=1, source_target_pairs={{0,3},{1,2},{2,1},{3,0},{4,7},{5,6},{6,5},{7,4},{8,11},{9,10},{10,... | collective-permute-start | bytes 196616 | tf_op jit(solution)/shard_map/ppermute | solution.py:58
  151.3 10.4 %copy-start.1 = (bf16[1,512,256]{2,1,0:T(8,128)(2,1)}, bf16[1,512,256]{2,1,0:T(8,128)(2,1)S(1)}, u32[]{:S(2)}) copy-start(bf16[1,512,256]{2,1,0:T(8,128)(2,1)S(1)} %dynamic_update_slice.15) | copy-start | bytes 786436
  151.3 3.1 %copy-start = (bf16[768,2048]{1,0:T(8,128)(2,1)S(1)}, bf16[768,2048]{1,0:T(8,128)(2,1)}, u32[]{:S(2)}) copy-start(bf16[768,2048]{1,0:T(8,128)(2,1)} %all-gather.2.cloned.1.call-done) | copy-start | bytes 9437188
  163.0 49.3 %copy-start.9 = (f32[128,2]{0,1:T(2,128)S(1)}, f32[128,2]{0,1:T(2,128)}, u32[]{:S(2)}) copy-start(f32[128,2]{0,1:T(2,128)} %param.12) | copy-start | bytes 3076
  163.0 51.4 %all-to-all-start.4 = ((bf16[8,96,512]{2,1,0:T(8,128)(2,1)}), bf16[8,96,512]{2,1,0:T(8,128)(2,1)}, u32[]{:S(2)}, u32[]{:S(2)}) async-start(bf16[8,96,512]{2,1,0:T(8,128)(2,1)} %bitcast.11), calls=%async_computation.5 | async-start | bytes 1572864 | tf_op jit(solution)/shard_map/all_to_all | solution.py:111
  167.3 64.6 %reduce-scatter.2.cloned.1.call-start = ((), (), s32[]{:S(2)}) async-start(), calls=%async_computation.6 | async-start | bytes 655360 | tf_op jit(solution)/shard_map/reduce_scatter | solution.py:78
Sparse Core Ops, SparseCore 0:
  50.3 27.1 all-gather.1
  212.4 19.4 reduce-scatter.1
